TPU v7x, 32 devices: a whole 2x2x4 slice. The times are simulated.
32 devices in a mesh: row: 8 (over z, y), col: 4 (over x, core).
Axes of the slice: x: 2, y: 2, z: 4, core: 2. Of those that a mesh axis runs over, the one named last changes fastest.
Arguments:
- tokens: bfloat16 [16384, 2048], P(('row', 'col')), may hold values from -6 to 6
- w_mix: bfloat16 [2048, 512], replicated, may hold values from -0.125 to 0.125
- w_gate: bfloat16 [2048, 2048], replicated, may hold values from -0.125 to 0.125
- gate_bias: float32 [2048], replicated, may hold values from -4 to 4
- w_branch: bfloat16 [512, 2048], replicated, may hold values from -0.25 to 0.25
Outputs:
- mixed: bfloat16 [16384, 2048], P(('row', 'col'))
All inputs are finite; a program needn't handle non-finite values.
Results may differ from a plain program's by a relative error of at most 0.0083.
Values may be sent and summed in bfloat16 or wider, within the bound.
A program may use at most 64 MiB of HBM per device.

v0:
```python
import functools
import math

import jax
import jax.numpy as jnp
import numpy as np
from jax import lax
from jax.experimental import pallas as pl
from jax.experimental.pallas import tpu as pltpu
from jax.sharding import PartitionSpec as P

GROUP_DIM = 64
HALF = GROUP_DIM // 2
UNIT = 16
ROWS = 8
BLOCK = 128
SPAN = 256
MESH = pl.DeviceIdType.MESH


def phases(left, right, period):
    angle = (left[:, None] * right[None, :] % period) * (2.0 * math.pi / period)
    return np.cos(angle), np.sin(angle)


def channel_tables(span):
    index = np.arange(GROUP_DIM)
    packed = np.where(index <= HALF, index, index - HALF)
    cos_c, sin_c = phases(packed, index, GROUP_DIM)
    is_sin = index > HALF
    forward = np.where(is_sin[:, None], sin_c, cos_c)
    back = np.zeros((GROUP_DIM, GROUP_DIM))
    for row in index:
        freq = packed[row]
        mirror = (GROUP_DIM - freq) % GROUP_DIM
        back[row, freq] += -1.0 if is_sin[row] else 1.0
        if mirror != freq:
            back[row, mirror] += 1.0
    copies = np.eye(span // GROUP_DIM)
    return np.kron(copies, forward).astype(jnp.bfloat16), np.kron(copies, back).astype(jnp.bfloat16)


def plain(tokens, w_mix, w_gate, gate_bias, w_branch):
    axes = ("row", "col")
    n_dev = lax.axis_size(axes)
    local_len, full_len = tokens.shape[0], tokens.shape[0] * n_dev
    sub_len = local_len // n_dev
    channels = w_mix.shape[1]
    cols = channels // n_dev
    forward, back = channel_tables(channels)
    mixed_in = jnp.dot(tokens, w_mix, preferred_element_type=jnp.float32).astype(jnp.bfloat16)
    packed = jnp.einsum("ab,nb->an", forward, mixed_in, preferred_element_type=jnp.float32)
    packed = packed.astype(jnp.bfloat16).reshape(n_dev, cols, local_len)
    packed = lax.all_to_all(packed, axes, split_axis=0, concat_axis=0, tiled=True)
    dev, pos = np.arange(n_dev), np.arange(local_len)
    cos_p, sin_p = (t.astype(jnp.bfloat16) for t in phases(dev, dev, n_dev))
    cos_t, sin_t = (jnp.asarray(t, jnp.float32)[:, None, :] for t in phases(dev, pos, full_len))
    cos_m, sin_m = (t.astype(jnp.bfloat16) for t in phases(pos, pos, local_len))
    first_re = jnp.einsum("kp,pcj->kcj", cos_p, packed, preferred_element_type=jnp.float32)
    first_im = -jnp.einsum("kp,pcj->kcj", sin_p, packed, preferred_element_type=jnp.float32)
    column = lax.axis_index(axes) * cols + jnp.arange(cols, dtype=jnp.int32)
    is_sin = (column % GROUP_DIM > HALF)[None, :, None]
    rot_c, rot_s = jnp.where(is_sin, sin_t, cos_t), jnp.where(is_sin, -cos_t, sin_t)
    part_re = (first_re * rot_c + first_im * rot_s).astype(jnp.bfloat16)
    part_im = (first_im * rot_c - first_re * rot_s).astype(jnp.bfloat16)
    real = jnp.einsum("kcj,jm->kcm", part_re, cos_m, preferred_element_type=jnp.float32)
    real = real + jnp.einsum("kcj,jm->kcm", part_im, sin_m, preferred_element_type=jnp.float32)
    real = (real * (1.0 / math.sqrt(full_len * GROUP_DIM))).astype(jnp.bfloat16)
    real = real.reshape(n_dev, cols, n_dev, sub_len).transpose(2, 1, 0, 3)
    real = lax.all_to_all(real, axes, split_axis=0, concat_axis=0, tiled=True)
    rows = real.transpose(3, 2, 0, 1).reshape(local_len, channels)
    turned = jnp.dot(back, w_branch, preferred_element_type=jnp.float32).astype(jnp.bfloat16)
    gate = jax.nn.sigmoid(jnp.dot(tokens, w_gate, preferred_element_type=jnp.float32) + gate_bias)
    return (gate * jnp.dot(rows, turned, preferred_element_type=jnp.float32)).astype(jnp.bfloat16)


def dot(a, b):
    return jnp.dot(a, b, preferred_element_type=jnp.float32)


def dot_t(a, b):
    return lax.dot_general(a, b, (((1,), (1,)), ((), ())), preferred_element_type=jnp.float32)


def swap_units(block):
    units = [block[ROWS * i : ROWS * (i + 1)] for i in range(BLOCK // UNIT)]
    lane = lax.broadcasted_iota(jnp.int32, (ROWS, BLOCK), 1) // UNIT
    for bit in range(3):
        step = 1 << bit
        low = (lane // step) % 2 == 0
        for i in range(len(units)):
            if i & step:
                continue
            a, b = units[i], units[i + step]
            units[i] = jnp.where(low, a, pltpu.roll(b, UNIT * step, 1))
            units[i + step] = jnp.where(low, pltpu.roll(a, BLOCK - UNIT * step, 1), b)
    return units


def kernel(
    n, n_col, scale,
    tok_hbm, wmix_hbm, wgate_hbm, bias_hbm, wbr_hbm,
    fwd_hbm, back_hbm, first_hbm, cos_hbm, sin_hbm, last_hbm, perm_hbm,
    gate, turned, rows,
    tok, wmix, wgate, bias_ref, wbr, fwd, back, first, cos_t, sin_t, last, perm,
    mixed,
    send1, recv1, send2, recv2,
    load_sem, s1_sem, r1_sem, s2_sem, r2_sem,
):
    me = lax.axis_index("row") * n_col + lax.axis_index("col")
    local_len, width = tok.shape
    channels = wmix.shape[1]

    pairs = (
        (tok_hbm, tok), (wmix_hbm, wmix), (fwd_hbm, fwd), (bias_hbm, bias_ref), (wgate_hbm, wgate),
        (first_hbm, first), (cos_hbm, cos_t), (sin_hbm, sin_t), (last_hbm, last),
        (wbr_hbm, wbr), (back_hbm, back), (perm_hbm, perm),
    )
    loads = [pltpu.make_async_copy(a, b, load_sem.at[i]) for i, (a, b) in enumerate(pairs)]
    for i in range(3):
        loads[i].start()

    barrier = pltpu.get_barrier_semaphore()

    def greet(r, carry):
        peer = (me + r) % n
        pl.semaphore_signal(barrier, inc=1, device_id=(peer // n_col, peer % n_col), device_id_type=MESH)
        return carry

    lax.fori_loop(1, n, greet, 0)

    for i in range(3):
        loads[i].wait()
    for i in range(3, len(loads)):
        loads[i].start()

    def mix(i, carry):
        at = pl.ds(pl.multiple_of(i * SPAN, SPAN), SPAN)
        mixed[at, :] = dot(tok[at, :], wmix[...]).astype(jnp.bfloat16)
        return carry

    lax.fori_loop(0, local_len // SPAN, mix, 0)
    for i in range(channels // SPAN):
        packed = dot_t(fwd[...], mixed[:, SPAN * i : SPAN * (i + 1)])
        send1[i] = packed.reshape(n, ROWS, local_len).astype(jnp.bfloat16)

    pl.semaphore_wait(barrier, n - 1)

    def remote(src, dst, s_sem, r_sem, h, peer, slot):
        return pltpu.make_async_remote_copy(
            src_ref=src.at[h, peer], dst_ref=dst.at[h, slot],
            send_sem=s_sem.at[h, peer], recv_sem=r_sem.at[h, slot],
            device_id=(peer // n_col, peer % n_col), device_id_type=MESH,
        )

    def each_peer(act):
        def step(r, carry):
            act((me + r) % n)
            return carry

        lax.fori_loop(1, n, step, 0)

    def own(src, dst, s_sem, r_sem, h):
        return pltpu.make_async_copy(src.at[h, me], dst.at[h, me], r_sem.at[h, me])

    def exchange(ex, h):
        each_peer(lambda peer: remote(*ex, h, peer, me).start())
        own(*ex, h).start()

    def arrived(ex, h):
        each_peer(lambda peer: remote(*ex, h, peer, peer).wait_recv())
        own(*ex, h).wait()

    def sent(ex, h):
        each_peer(lambda peer: remote(*ex, h, peer, me).wait_send())

    one = (send1, recv1, s1_sem, r1_sem)
    two = (send2, recv2, s2_sem, r2_sem)
    exchange(one, 0)
    exchange(one, 1)

    loads[3].wait()
    loads[4].wait()

    def open_gate(i, carry):
        at = pl.ds(pl.multiple_of(i * SPAN, SPAN), SPAN)
        gate[:, at] = jax.nn.sigmoid(dot(tok[...], wgate[:, at]) + bias_ref[:, at])
        return carry

    lax.fori_loop(0, width // SPAN, open_gate, 0)
    for i in range(5, len(loads)):
        loads[i].wait()

    chunk = n * ROWS
    per = BLOCK // UNIT
    blocks = n // per

    def matrix(block):
        return block.astype(jnp.float32).reshape(chunk, local_len).astype(jnp.bfloat16)

    for h in range(2):
        column = h * chunk + me * ROWS + lax.broadcasted_iota(jnp.int32, (1, ROWS, local_len), 1)
        is_sin = column % GROUP_DIM > HALF
        arrived(one, h)
        gathered = matrix(recv1[h])
        first_re = dot(first[:chunk, :], gathered).reshape(n, ROWS, local_len)
        first_im = dot(first[chunk:, :], gathered).reshape(n, ROWS, local_len)
        c = jnp.broadcast_to(cos_t[...].reshape(n, 1, local_len), (n, ROWS, local_len))
        s = jnp.broadcast_to(sin_t[...].reshape(n, 1, local_len), (n, ROWS, local_len))
        c, s = jnp.where(is_sin, s, c), jnp.where(is_sin, -c, s)
        part_re = (first_re * c + first_im * s).reshape(chunk, local_len).astype(jnp.bfloat16)
        part_im = (first_im * c - first_re * s).reshape(chunk, local_len).astype(jnp.bfloat16)
        real = (dot(part_re, last[:local_len, :]) + dot(part_im, last[local_len:, :])) * scale
        for a in range(blocks):
            for b in range(blocks):
                block = real[ROWS * per * a : ROWS * per * (a + 1), BLOCK * b : BLOCK * (b + 1)]
                for i, unit in enumerate(swap_units(block)):
                    send2[h, per * b + i, :, BLOCK * a : BLOCK * (a + 1)] = unit.astype(jnp.bfloat16)
        exchange(two, h)

    def turn(j, carry):
        lanes = pl.ds(pl.multiple_of(j * SPAN, SPAN), SPAN)
        for i in range(channels // SPAN):
            at = slice(SPAN * i, SPAN * (i + 1))
            turned[at, lanes] = dot(back[...], wbr[at, lanes]).astype(jnp.bfloat16)
        return carry

    lax.fori_loop(0, width // SPAN, turn, 0)
    sent(one, 0)
    sent(one, 1)
    for h in range(2):
        arrived(two, h)
        rows[:, chunk * h : chunk * (h + 1)] = dot_t(perm[...], matrix(recv2[h])).astype(jnp.bfloat16)
    sent(two, 0)
    sent(two, 1)


def fused(tokens, w_mix, w_gate, gate_bias, w_branch):
    axes = ("row", "col")
    n_dev = lax.axis_size(axes)
    n_col = lax.axis_size("col")
    local_len, width = tokens.shape
    channels = w_mix.shape[1]
    full_len = local_len * n_dev
    bf16, f32 = jnp.bfloat16, jnp.float32

    dev, pos = np.arange(n_dev), np.arange(local_len)
    forward, back = channel_tables(SPAN)
    cos_p, sin_p = phases(dev, dev, n_dev)
    unit = np.eye(ROWS)
    first = np.concatenate([np.kron(cos_p, unit), np.kron(-sin_p, unit)]).astype(bf16)
    cos_t, sin_t = (t.astype(np.float32) for t in phases(dev, pos, full_len))
    last = np.concatenate(phases(pos, pos, local_len)).astype(bf16)
    order = (pos % n_dev) * UNIT + pos // n_dev
    perm = np.eye(local_len)[order].astype(bf16)

    tables = [forward, back, first, cos_t, sin_t, last, perm]
    any_space = pl.BlockSpec(memory_space=pl.ANY)
    block = pltpu.VMEM((2, n_dev, ROWS, local_len), bf16)
    sems = pltpu.SemaphoreType.DMA((2, n_dev))
    vmem = lambda array: pltpu.VMEM(array.shape, array.dtype)
    gate, turned, rows = pl.pallas_call(
        functools.partial(kernel, n_dev, n_col, 1.0 / math.sqrt(full_len * GROUP_DIM)),
        out_shape=[
            pltpu.VMEM((local_len, width), f32),
            pltpu.VMEM((channels, width), bf16),
            pltpu.VMEM((local_len, channels), bf16),
        ],
        in_specs=[any_space] * 12,
        out_specs=[pl.BlockSpec(memory_space=pltpu.VMEM)] * 3,
        scratch_shapes=[
            vmem(tokens), vmem(w_mix), vmem(w_gate), pltpu.VMEM((1, width), f32), vmem(w_branch),
            vmem(forward), vmem(back), vmem(first), vmem(cos_t), vmem(sin_t), vmem(last), vmem(perm),
            pltpu.VMEM((local_len, channels), bf16),
            block, block, block, block,
            pltpu.SemaphoreType.DMA((12,)),
            sems, sems, sems, sems,
        ],
        compiler_params=pltpu.CompilerParams(
            collective_id=0, has_side_effects=True, vmem_limit_bytes=56 * 1024 * 1024
        ),
    )(tokens, w_mix, w_gate, gate_bias.reshape(1, width), w_branch, *[jnp.asarray(t) for t in tables])
    return (gate * dot(rows, turned)).astype(bf16)


def shards(tokens, w_mix, w_gate, gate_bias, w_branch):
    n_dev = lax.axis_size(("row", "col"))
    local_len, channels = tokens.shape[0], w_mix.shape[1]
    tiled = n_dev * ROWS == SPAN and channels == 2 * SPAN and local_len == n_dev * UNIT
    step = fused if tiled else plain
    return step(tokens, w_mix, w_gate, gate_bias, w_branch)


def solution(mesh):
    in_specs = (P(("row", "col"), None), P(), P(), P(), P())
    out_specs = P(("row", "col"), None)
    return jax.shard_map(shards, mesh=mesh, in_specs=in_specs, out_specs=out_specs, check_vma=False)
```

profile of v0, /device:TPU:9, one launch (start us, length us, event | category | flops | bytes accessed | tf_op | source)
XLA Modules:
  0.0 36.6 jit_solution(3060429884902789199)
XLA Ops:
  0.0 34.0 %shard_map.118 = (f32[512,2048]{1,0:T(8,128)S(1)}, bf16[512,2048]{1,0:T(8,128)(2,1)S(1)}, bf16[512,512]{1,0:T(8,128)(2,1)S(1)}) custom-call(bf16[512,2048]{1,0:T(8,128)(2,1)} %tok_hbm.1, bf16[2048,512]{1,0:T(8,128)(2,1)} %wmix_hbm.1, bf16[2048,2048]{1,0:T(8,128)(2,1)} %wgate_hbm.1, f32[1,2048]{1,0:T(1,128)} %bitcast.3, bf16[512,2048]{1,0:T(8,128)(2,1)} %wbr_hbm.1, ...), custom_call_target="tpu_custom_call" | custom-call | tf_op jit(solution)/shard_map/pallas_call | solution.py:262
  34.0 2.6 %multiply_convert_fusion = bf16[512,2048]{1,0:T(8,128)(2,1)} fusion(f32[512,2048]{1,0:T(8,128)S(1)} %get-tuple-element.8, bf16[512,512]{1,0:T(8,128)(2,1)S(1)} %get-tuple-element.9, bf16[512,2048]{1,0:T(8,128)(2,1)S(1)} %get-tuple-element.10), kind=kOutput, calls=%fused_computation | convolution fusion | flops 1075838976 | bytes 8912896 | tf_op jit(solution)/shard_map/dot_general | solution.py:78
where the time goes:
time: 36.9 us; the launch traced here: 36.6 us
  Pallas kernels  34 us (92%)
  matrix products  2.58 us (7%)
    pallas_call x1, Pallas kernels, fused(): pl.pallas_call(functools.partial(kernel, n_dev, n_col, 1.0 / math.sqrt(fu...  34 us
    dot_general x1, matrix products, dot(): return jnp.dot(a, b, preferred_element_type=jnp.float32)  2.58 us

commit v1 on v0

--- a/solution.py
+++ b/solution.py
@@ -101,23 +101,28 @@
     n, n_col, scale,
     tok_hbm, wmix_hbm, wgate_hbm, bias_hbm, wbr_hbm,
     fwd_hbm, back_hbm, first_hbm, cos_hbm, sin_hbm, last_hbm, perm_hbm,
-    gate, turned, rows,
+    gate, partial, turned_b, rows_b,
     tok, wmix, wgate, bias_ref, wbr, fwd, back, first, cos_t, sin_t, last, perm,
-    mixed,
+    mixed, turned_a, rows_a,
     send1, recv1, send2, recv2,
     load_sem, s1_sem, r1_sem, s2_sem, r2_sem,
 ):
     me = lax.axis_index("row") * n_col + lax.axis_index("col")
     local_len, width = tok.shape
-    channels = wmix.shape[1]
+    channels = mixed.shape[1]
+    half_len = local_len // 2
 
     pairs = (
-        (tok_hbm, tok), (wmix_hbm, wmix), (fwd_hbm, fwd), (bias_hbm, bias_ref), (wgate_hbm, wgate),
+        (wmix_hbm.at[:, pl.ds(0, SPAN)], wmix.at[0]),
+        (tok_hbm.at[pl.ds(0, half_len)], tok.at[pl.ds(0, half_len)]),
+        (tok_hbm.at[pl.ds(half_len, half_len)], tok.at[pl.ds(half_len, half_len)]),
+        (fwd_hbm, fwd), (wmix_hbm.at[:, pl.ds(SPAN, SPAN)], wmix.at[1]),
+        (bias_hbm, bias_ref), (wgate_hbm, wgate),
         (first_hbm, first), (cos_hbm, cos_t), (sin_hbm, sin_t), (last_hbm, last),
         (wbr_hbm, wbr), (back_hbm, back), (perm_hbm, perm),
     )
     loads = [pltpu.make_async_copy(a, b, load_sem.at[i]) for i, (a, b) in enumerate(pairs)]
-    for i in range(3):
+    for i in range(5):
         loads[i].start()
 
     barrier = pltpu.get_barrier_semaphore()
@@ -128,23 +133,6 @@
         return carry
 
     lax.fori_loop(1, n, greet, 0)
-
-    for i in range(3):
-        loads[i].wait()
-    for i in range(3, len(loads)):
-        loads[i].start()
-
-    def mix(i, carry):
-        at = pl.ds(pl.multiple_of(i * SPAN, SPAN), SPAN)
-        mixed[at, :] = dot(tok[at, :], wmix[...]).astype(jnp.bfloat16)
-        return carry
-
-    lax.fori_loop(0, local_len // SPAN, mix, 0)
-    for i in range(channels // SPAN):
-        packed = dot_t(fwd[...], mixed[:, SPAN * i : SPAN * (i + 1)])
-        send1[i] = packed.reshape(n, ROWS, local_len).astype(jnp.bfloat16)
-
-    pl.semaphore_wait(barrier, n - 1)
 
     def remote(src, dst, s_sem, r_sem, h, peer, slot):
         return pltpu.make_async_remote_copy(
@@ -176,11 +164,32 @@
 
     one = (send1, recv1, s1_sem, r1_sem)
     two = (send2, recv2, s2_sem, r2_sem)
+
+    def pack(h):
+        packed = dot_t(fwd[...], mixed[:, SPAN * h : SPAN * (h + 1)])
+        send1[h] = packed.reshape(n, ROWS, local_len).astype(jnp.bfloat16)
+
+    loads[0].wait()
+    for i in range(2):
+        at = slice(half_len * i, half_len * (i + 1))
+        loads[1 + i].wait()
+        mixed[at, :SPAN] = dot(tok[at, :], wmix[0]).astype(jnp.bfloat16)
+    loads[3].wait()
+    pack(0)
+    pl.semaphore_wait(barrier, n - 1)
     exchange(one, 0)
+
+    for i in range(5, len(loads)):
+        loads[i].start()
+    loads[4].wait()
+    for i in range(2):
+        at = slice(half_len * i, half_len * (i + 1))
+        mixed[at, SPAN:] = dot(tok[at, :], wmix[1]).astype(jnp.bfloat16)
+    pack(1)
     exchange(one, 1)
 
-    loads[3].wait()
-    loads[4].wait()
+    loads[5].wait()
+    loads[6].wait()
 
     def open_gate(i, carry):
         at = pl.ds(pl.multiple_of(i * SPAN, SPAN), SPAN)
@@ -188,7 +197,7 @@
         return carry
 
     lax.fori_loop(0, width // SPAN, open_gate, 0)
-    for i in range(5, len(loads)):
+    for i in range(7, len(loads)):
         loads[i].wait()
 
     chunk = n * ROWS
@@ -197,6 +206,14 @@
 
     def matrix(block):
         return block.astype(jnp.float32).reshape(chunk, local_len).astype(jnp.bfloat16)
+
+    def turn(h, out):
+        def step(j, carry):
+            lanes = pl.ds(pl.multiple_of(j * SPAN, SPAN), SPAN)
+            out[:, lanes] = dot(back[...], wbr[SPAN * h : SPAN * (h + 1), lanes]).astype(jnp.bfloat16)
+            return carry
+
+        lax.fori_loop(0, width // SPAN, step, 0)
 
     for h in range(2):
         column = h * chunk + me * ROWS + lax.broadcasted_iota(jnp.int32, (1, ROWS, local_len), 1)
@@ -217,21 +234,24 @@
                 for i, unit in enumerate(swap_units(block)):
                     send2[h, per * b + i, :, BLOCK * a : BLOCK * (a + 1)] = unit.astype(jnp.bfloat16)
         exchange(two, h)
-
-    def turn(j, carry):
-        lanes = pl.ds(pl.multiple_of(j * SPAN, SPAN), SPAN)
-        for i in range(channels // SPAN):
-            at = slice(SPAN * i, SPAN * (i + 1))
-            turned[at, lanes] = dot(back[...], wbr[at, lanes]).astype(jnp.bfloat16)
-        return carry
-
-    lax.fori_loop(0, width // SPAN, turn, 0)
+        if h == 0:
+            turn(0, turned_a)
+
+    turn(1, turned_b)
     sent(one, 0)
     sent(one, 1)
-    for h in range(2):
-        arrived(two, h)
-        rows[:, chunk * h : chunk * (h + 1)] = dot_t(perm[...], matrix(recv2[h])).astype(jnp.bfloat16)
+    arrived(two, 0)
+    rows_a[...] = dot_t(perm[...], matrix(recv2[0])).astype(jnp.bfloat16)
+
+    def first_half(j, carry):
+        lanes = pl.ds(pl.multiple_of(j * SPAN, SPAN), SPAN)
+        partial[:, lanes] = gate[:, lanes] * dot(rows_a[...], turned_a[:, lanes])
+        return carry
+
+    lax.fori_loop(0, width // SPAN, first_half, 0)
     sent(two, 0)
+    arrived(two, 1)
+    rows_b[...] = dot_t(perm[...], matrix(recv2[1])).astype(jnp.bfloat16)
     sent(two, 1)
 
 
@@ -259,28 +279,31 @@
     block = pltpu.VMEM((2, n_dev, ROWS, local_len), bf16)
     sems = pltpu.SemaphoreType.DMA((2, n_dev))
     vmem = lambda array: pltpu.VMEM(array.shape, array.dtype)
-    gate, turned, rows = pl.pallas_call(
+    gate, partial, turned, rows = pl.pallas_call(
         functools.partial(kernel, n_dev, n_col, 1.0 / math.sqrt(full_len * GROUP_DIM)),
         out_shape=[
             pltpu.VMEM((local_len, width), f32),
-            pltpu.VMEM((channels, width), bf16),
-            pltpu.VMEM((local_len, channels), bf16),
+            pltpu.VMEM((local_len, width), f32),
+            pltpu.VMEM((SPAN, width), bf16),
+            pltpu.VMEM((local_len, SPAN), bf16),
         ],
         in_specs=[any_space] * 12,
-        out_specs=[pl.BlockSpec(memory_space=pltpu.VMEM)] * 3,
+        out_specs=[pl.BlockSpec(memory_space=pltpu.VMEM)] * 4,
         scratch_shapes=[
-            vmem(tokens), vmem(w_mix), vmem(w_gate), pltpu.VMEM((1, width), f32), vmem(w_branch),
+            vmem(tokens), pltpu.VMEM((2, width, SPAN), bf16), vmem(w_gate), pltpu.VMEM((1, width), f32), vmem(w_branch),
             vmem(forward), vmem(back), vmem(first), vmem(cos_t), vmem(sin_t), vmem(last), vmem(perm),
             pltpu.VMEM((local_len, channels), bf16),
+            pltpu.VMEM((SPAN, width), bf16),
+            pltpu.VMEM((local_len, SPAN), bf16),
             block, block, block, block,
-            pltpu.SemaphoreType.DMA((12,)),
+            pltpu.SemaphoreType.DMA((14,)),
             sems, sems, sems, sems,
         ],
         compiler_params=pltpu.CompilerParams(
-            collective_id=0, has_side_effects=True, vmem_limit_bytes=56 * 1024 * 1024
+            collective_id=0, has_side_effects=True, vmem_limit_bytes=57_200_000
         ),
     )(tokens, w_mix, w_gate, gate_bias.reshape(1, width), w_branch, *[jnp.asarray(t) for t in tables])
-    return (gate * dot(rows, turned)).astype(bf16)
+    return (partial + gate * dot(rows, turned)).astype(bf16)
 
 
 def shards(tokens, w_mix, w_gate, gate_bias, w_branch):

time: 36.9 us -> 36 us (0.976)
  the two profiles are of different devices: /device:TPU:9 before, /device:TPU:0 now
where the time goes in v1:
time: 36 us; the launch traced here: 35.9 us
  Pallas kernels  33.8 us (94%)
  matrix products  2.04 us (6%)
    pallas_call x1, Pallas kernels, fused(): pl.pallas_call(functools.partial(kernel, n_dev, n_col, 1.0 / math.sqrt(fu...  33.8 us
    dot_general x1, matrix products, dot(): return jnp.dot(a, b, preferred_element_type=jnp.float32)  2.04 us

profile of v1, /device:TPU:0, one launch (start us, length us, event | category | flops | bytes accessed | tf_op | source)
XLA Modules:
  0.0 35.9 jit_solution(13168796476912937299)
XLA Ops:
  0.0 33.8 %shard_map.118 = (f32[512,2048]{1,0:T(8,128)S(1)}, f32[512,2048]{1,0:T(8,128)S(1)}, bf16[256,2048]{1,0:T(8,128)(2,1)S(1)}, bf16[512,256]{1,0:T(8,128)(2,1)S(1)}) custom-call(bf16[512,2048]{1,0:T(8,128)(2,1)} %tok_hbm.1, bf16[2048,512]{1,0:T(8,128)(2,1)} %wmix_hbm.1, bf16[2048,2048]{1,0:T(8,128)(2,1)} %wgate_hbm.1, f32[1,2048]{1,0:T(1,128)} %bitcast.3, ...), custom_call_target="tpu_custom_call" | custom-call | tf_op jit(solution)/shard_map/pallas_call | solution.py:282
  33.8 2.0 %add_convert_fusion = bf16[512,2048]{1,0:T(8,128)(2,1)} fusion(f32[512,2048]{1,0:T(8,128)S(1)} %get-tuple-element.9, f32[512,2048]{1,0:T(8,128)S(1)} %get-tuple-element.10, bf16[512,256]{1,0:T(8,128)(2,1)S(1)} %get-tuple-element.11, bf16[256,2048]{1,0:T(8,128)(2,1)S(1)} %get-tuple-element.12), kind=kOutput, calls=%fused_computation | convolution fusion | flops 540016640 | bytes 11796480 | tf_op jit(solution)/shard_map/dot_general | solution.py:78

commit v2 on v1

--- a/solution.py
+++ b/solution.py
@@ -108,8 +108,8 @@
     load_sem, s1_sem, r1_sem, s2_sem, r2_sem,
 ):
     me = lax.axis_index("row") * n_col + lax.axis_index("col")
+    chip, core, owners = me // 2, me % 2, n // 2
     local_len, width = tok.shape
-    channels = mixed.shape[1]
     half_len = local_len // 2
 
     pairs = (
@@ -134,12 +134,48 @@
 
     lax.fori_loop(1, n, greet, 0)
 
-    def remote(src, dst, s_sem, r_sem, h, peer, slot):
+    def device(dev):
+        return (dev // n_col, dev % n_col)
+
+    def to_owner(h, i):
         return pltpu.make_async_remote_copy(
-            src_ref=src.at[h, peer], dst_ref=dst.at[h, slot],
-            send_sem=s_sem.at[h, peer], recv_sem=r_sem.at[h, slot],
-            device_id=(peer // n_col, peer % n_col), device_id_type=MESH,
+            src_ref=send1.at[h, i], dst_ref=recv1.at[me],
+            send_sem=s1_sem.at[h, i], recv_sem=r1_sem.at[me],
+            device_id=device(2 * i + h), device_id_type=MESH,
         )
+
+    def from_source(dev):
+        return pltpu.make_async_remote_copy(
+            src_ref=send1.at[0, 0], dst_ref=recv1.at[dev],
+            send_sem=s1_sem.at[0, 0], recv_sem=r1_sem.at[dev],
+            device_id=device(dev), device_id_type=MESH,
+        )
+
+    def to_reader(dev):
+        return pltpu.make_async_remote_copy(
+            src_ref=send2.at[dev], dst_ref=recv2.at[core, chip],
+            send_sem=s2_sem.at[dev], recv_sem=r2_sem.at[core, chip],
+            device_id=device(dev), device_id_type=MESH,
+        )
+
+    def from_owner(h, i):
+        return pltpu.make_async_remote_copy(
+            src_ref=send2.at[0], dst_ref=recv2.at[h, i],
+            send_sem=s2_sem.at[0], recv_sem=r2_sem.at[h, i],
+            device_id=device(2 * i + h), device_id_type=MESH,
+        )
+
+    def each_owner(h, act):
+        def step(r, carry):
+            i = chip ^ ((r + 8) % owners)
+
+            @pl.when(2 * i + h != me)
+            def _():
+                act(h, i)
+
+            return carry
+
+        lax.fori_loop(0, owners, step, 0)
 
     def each_peer(act):
         def step(r, carry):
@@ -148,26 +184,9 @@
 
         lax.fori_loop(1, n, step, 0)
 
-    def own(src, dst, s_sem, r_sem, h):
-        return pltpu.make_async_copy(src.at[h, me], dst.at[h, me], r_sem.at[h, me])
-
-    def exchange(ex, h):
-        each_peer(lambda peer: remote(*ex, h, peer, me).start())
-        own(*ex, h).start()
-
-    def arrived(ex, h):
-        each_peer(lambda peer: remote(*ex, h, peer, peer).wait_recv())
-        own(*ex, h).wait()
-
-    def sent(ex, h):
-        each_peer(lambda peer: remote(*ex, h, peer, me).wait_send())
-
-    one = (send1, recv1, s1_sem, r1_sem)
-    two = (send2, recv2, s2_sem, r2_sem)
-
     def pack(h):
         packed = dot_t(fwd[...], mixed[:, SPAN * h : SPAN * (h + 1)])
-        send1[h] = packed.reshape(n, ROWS, local_len).astype(jnp.bfloat16)
+        send1[h] = packed.reshape(owners, UNIT, local_len).astype(jnp.bfloat16)
 
     loads[0].wait()
     for i in range(2):
@@ -177,7 +196,7 @@
     loads[3].wait()
     pack(0)
     pl.semaphore_wait(barrier, n - 1)
-    exchange(one, 0)
+    each_owner(0, lambda h, i: to_owner(h, i).start())
 
     for i in range(5, len(loads)):
         loads[i].start()
@@ -186,7 +205,7 @@
         at = slice(half_len * i, half_len * (i + 1))
         mixed[at, SPAN:] = dot(tok[at, :], wmix[1]).astype(jnp.bfloat16)
     pack(1)
-    exchange(one, 1)
+    recv1[me] = send1[core, chip]
 
     loads[5].wait()
     loads[6].wait()
@@ -196,16 +215,12 @@
         gate[:, at] = jax.nn.sigmoid(dot(tok[...], wgate[:, at]) + bias_ref[:, at])
         return carry
 
-    lax.fori_loop(0, width // SPAN, open_gate, 0)
+    lax.fori_loop(0, 3, open_gate, 0)
+    each_owner(1, lambda h, i: to_owner(h, i).start())
+    early = jnp.where(core == 0, 4, width // SPAN)
+    lax.fori_loop(3, early, open_gate, 0)
     for i in range(7, len(loads)):
         loads[i].wait()
-
-    chunk = n * ROWS
-    per = BLOCK // UNIT
-    blocks = n // per
-
-    def matrix(block):
-        return block.astype(jnp.float32).reshape(chunk, local_len).astype(jnp.bfloat16)
 
     def turn(h, out):
         def step(j, carry):
@@ -215,33 +230,42 @@
 
         lax.fori_loop(0, width // SPAN, step, 0)
 
-    for h in range(2):
-        column = h * chunk + me * ROWS + lax.broadcasted_iota(jnp.int32, (1, ROWS, local_len), 1)
-        is_sin = column % GROUP_DIM > HALF
-        arrived(one, h)
-        gathered = matrix(recv1[h])
+    chunk = n * ROWS
+    per = BLOCK // UNIT
+    blocks = n // per
+    column = core * SPAN + chip * UNIT + lax.broadcasted_iota(jnp.int32, (1, UNIT, local_len), 1)
+    is_sin = column % GROUP_DIM > HALF
+    c = jnp.broadcast_to(cos_t[...].reshape(n, 1, local_len), (n, ROWS, local_len))
+    s = jnp.broadcast_to(sin_t[...].reshape(n, 1, local_len), (n, ROWS, local_len))
+
+    each_peer(lambda peer: from_source(peer).wait_recv())
+    for half in range(2):
+        at = slice(ROWS * half, ROWS * (half + 1))
+        gathered = recv1[...].astype(jnp.float32)[:, at, :].reshape(chunk, local_len).astype(jnp.bfloat16)
         first_re = dot(first[:chunk, :], gathered).reshape(n, ROWS, local_len)
         first_im = dot(first[chunk:, :], gathered).reshape(n, ROWS, local_len)
-        c = jnp.broadcast_to(cos_t[...].reshape(n, 1, local_len), (n, ROWS, local_len))
-        s = jnp.broadcast_to(sin_t[...].reshape(n, 1, local_len), (n, ROWS, local_len))
-        c, s = jnp.where(is_sin, s, c), jnp.where(is_sin, -c, s)
-        part_re = (first_re * c + first_im * s).reshape(chunk, local_len).astype(jnp.bfloat16)
-        part_im = (first_im * c - first_re * s).reshape(chunk, local_len).astype(jnp.bfloat16)
+        turn_c, turn_s = jnp.where(is_sin[:, at, :], s, c), jnp.where(is_sin[:, at, :], -c, s)
+        part_re = (first_re * turn_c + first_im * turn_s).reshape(chunk, local_len).astype(jnp.bfloat16)
+        part_im = (first_im * turn_c - first_re * turn_s).reshape(chunk, local_len).astype(jnp.bfloat16)
         real = (dot(part_re, last[:local_len, :]) + dot(part_im, last[local_len:, :])) * scale
         for a in range(blocks):
             for b in range(blocks):
                 block = real[ROWS * per * a : ROWS * per * (a + 1), BLOCK * b : BLOCK * (b + 1)]
                 for i, unit in enumerate(swap_units(block)):
-                    send2[h, per * b + i, :, BLOCK * a : BLOCK * (a + 1)] = unit.astype(jnp.bfloat16)
-        exchange(two, h)
-        if h == 0:
-            turn(0, turned_a)
-
+                    send2[per * b + i, at, BLOCK * a : BLOCK * (a + 1)] = unit.astype(jnp.bfloat16)
+    each_peer(lambda peer: to_reader(peer).start())
+    recv2[core, chip] = send2[me]
+    lax.fori_loop(early, width // SPAN, open_gate, 0)
+    turn(0, turned_a)
     turn(1, turned_b)
-    sent(one, 0)
-    sent(one, 1)
-    arrived(two, 0)
-    rows_a[...] = dot_t(perm[...], matrix(recv2[0])).astype(jnp.bfloat16)
+
+    def rows(h):
+        each_owner(h, lambda h, i: from_owner(h, i).wait_recv())
+        return dot_t(perm[...], recv2[h].reshape(SPAN, local_len)).astype(jnp.bfloat16)
+
+    each_owner(0, lambda h, i: to_owner(h, i).wait_send())
+    each_owner(1, lambda h, i: to_owner(h, i).wait_send())
+    rows_a[...] = rows(0)
 
     def first_half(j, carry):
         lanes = pl.ds(pl.multiple_of(j * SPAN, SPAN), SPAN)
@@ -249,10 +273,8 @@
         return carry
 
     lax.fori_loop(0, width // SPAN, first_half, 0)
-    sent(two, 0)
-    arrived(two, 1)
-    rows_b[...] = dot_t(perm[...], matrix(recv2[1])).astype(jnp.bfloat16)
-    sent(two, 1)
+    each_peer(lambda peer: to_reader(peer).wait_send())
+    rows_b[...] = rows(1)
 
 
 def fused(tokens, w_mix, w_gate, gate_bias, w_branch):
@@ -276,8 +298,10 @@
 
     tables = [forward, back, first, cos_t, sin_t, last, perm]
     any_space = pl.BlockSpec(memory_space=pl.ANY)
-    block = pltpu.VMEM((2, n_dev, ROWS, local_len), bf16)
-    sems = pltpu.SemaphoreType.DMA((2, n_dev))
+    by_owner = pltpu.VMEM((2, n_dev // 2, UNIT, local_len), bf16)
+    by_device = pltpu.VMEM((n_dev, UNIT, local_len), bf16)
+    owner_sems = pltpu.SemaphoreType.DMA((2, n_dev // 2))
+    device_sems = pltpu.SemaphoreType.DMA((n_dev,))
     vmem = lambda array: pltpu.VMEM(array.shape, array.dtype)
     gate, partial, turned, rows = pl.pallas_call(
         functools.partial(kernel, n_dev, n_col, 1.0 / math.sqrt(full_len * GROUP_DIM)),
@@ -295,9 +319,9 @@
             pltpu.VMEM((local_len, channels), bf16),
             pltpu.VMEM((SPAN, width), bf16),
             pltpu.VMEM((local_len, SPAN), bf16),
-            block, block, block, block,
+            by_owner, by_device, by_device, by_owner,
             pltpu.SemaphoreType.DMA((14,)),
-            sems, sems, sems, sems,
+            owner_sems, device_sems, device_sems, owner_sems,
         ],
         compiler_params=pltpu.CompilerParams(
             collective_id=0, has_side_effects=True, vmem_limit_bytes=57_200_000

time: 36 us -> 34.3 us (0.953)
  the two profiles are of different devices: /device:TPU:0 before, /device:TPU:9 now
where the time goes in v2:
time: 34.3 us; the launch traced here: 34.2 us
  Pallas kernels  32.1 us (94%)
  matrix products  2.04 us (6%)
    pallas_call x1, Pallas kernels, fused(): pl.pallas_call(functools.partial(kernel, n_dev, n_col, 1.0 / math.sqrt(fu...  32.1 us
    dot_general x1, matrix products, dot(): return jnp.dot(a, b, preferred_element_type=jnp.float32)  2.04 us

profile of v2, /device:TPU:9, one launch (start us, length us, event | category | flops | bytes accessed | tf_op | source)
XLA Modules:
  0.0 34.2 jit_solution(10287382799775485455)
XLA Ops:
  0.0 32.1 %shard_map.118 = (f32[512,2048]{1,0:T(8,128)S(1)}, f32[512,2048]{1,0:T(8,128)S(1)}, bf16[256,2048]{1,0:T(8,128)(2,1)S(1)}, bf16[512,256]{1,0:T(8,128)(2,1)S(1)}) custom-call(bf16[512,2048]{1,0:T(8,128)(2,1)} %tok_hbm.1, bf16[2048,512]{1,0:T(8,128)(2,1)} %wmix_hbm.1, bf16[2048,2048]{1,0:T(8,128)(2,1)} %wgate_hbm.1, f32[1,2048]{1,0:T(1,128)} %bitcast.3, ...), custom_call_target="tpu_custom_call" | custom-call | tf_op jit(solution)/shard_map/pallas_call | solution.py:306
  32.2 2.0 %add_convert_fusion = bf16[512,2048]{1,0:T(8,128)(2,1)} fusion(f32[512,2048]{1,0:T(8,128)S(1)} %get-tuple-element.9, f32[512,2048]{1,0:T(8,128)S(1)} %get-tuple-element.10, bf16[512,256]{1,0:T(8,128)(2,1)S(1)} %get-tuple-element.11, bf16[256,2048]{1,0:T(8,128)(2,1)S(1)} %get-tuple-element.12), kind=kOutput, calls=%fused_computation | convolution fusion | flops 540016640 | bytes 11796480 | tf_op jit(solution)/shard_map/dot_general | solution.py:78

commit v3 on v2

--- a/solution.py
+++ b/solution.py
@@ -15,6 +15,7 @@
 ROWS = 8
 BLOCK = 128
 SPAN = 256
+FINISH = 8 * 1024 * 1024
 MESH = pl.DeviceIdType.MESH
 
 
@@ -101,9 +102,9 @@
     n, n_col, scale,
     tok_hbm, wmix_hbm, wgate_hbm, bias_hbm, wbr_hbm,
     fwd_hbm, back_hbm, first_hbm, cos_hbm, sin_hbm, last_hbm, perm_hbm,
-    gate, partial, turned_b, rows_b,
+    gate, partial, turned_a, turned_b, rows_a, rows_b,
     tok, wmix, wgate, bias_ref, wbr, fwd, back, first, cos_t, sin_t, last, perm,
-    mixed, turned_a, rows_a,
+    mixed,
     send1, recv1, send2, recv2,
     load_sem, s1_sem, r1_sem, s2_sem, r2_sem,
 ):
@@ -122,7 +123,7 @@
         (wbr_hbm, wbr), (back_hbm, back), (perm_hbm, perm),
     )
     loads = [pltpu.make_async_copy(a, b, load_sem.at[i]) for i, (a, b) in enumerate(pairs)]
-    for i in range(5):
+    for i in range(4):
         loads[i].start()
 
     barrier = pltpu.get_barrier_semaphore()
@@ -167,7 +168,7 @@
 
     def each_owner(h, act):
         def step(r, carry):
-            i = chip ^ ((r + 8) % owners)
+            i = chip ^ ((r + 3 * owners // 4) % owners)
 
             @pl.when(2 * i + h != me)
             def _():
@@ -193,6 +194,7 @@
         at = slice(half_len * i, half_len * (i + 1))
         loads[1 + i].wait()
         mixed[at, :SPAN] = dot(tok[at, :], wmix[0]).astype(jnp.bfloat16)
+    loads[4].start()
     loads[3].wait()
     pack(0)
     pl.semaphore_wait(barrier, n - 1)
@@ -215,10 +217,10 @@
         gate[:, at] = jax.nn.sigmoid(dot(tok[...], wgate[:, at]) + bias_ref[:, at])
         return carry
 
-    lax.fori_loop(0, 3, open_gate, 0)
+    lax.fori_loop(0, 2, open_gate, 0)
     each_owner(1, lambda h, i: to_owner(h, i).start())
-    early = jnp.where(core == 0, 4, width // SPAN)
-    lax.fori_loop(3, early, open_gate, 0)
+    early = jnp.where(core == 0, 3, width // SPAN)
+    lax.fori_loop(2, early, open_gate, 0)
     for i in range(7, len(loads)):
         loads[i].wait()
 
@@ -267,14 +269,25 @@
     each_owner(1, lambda h, i: to_owner(h, i).wait_send())
     rows_a[...] = rows(0)
 
-    def first_half(j, carry):
-        lanes = pl.ds(pl.multiple_of(j * SPAN, SPAN), SPAN)
-        partial[:, lanes] = gate[:, lanes] * dot(rows_a[...], turned_a[:, lanes])
-        return carry
-
-    lax.fori_loop(0, width // SPAN, first_half, 0)
+    for j in range(8):
+        at = slice(SPAN * j, SPAN * (j + 1))
+        partial[:, at] = dot(rows_a[...], turned_a[:, at])
     each_peer(lambda peer: to_reader(peer).wait_send())
     rows_b[...] = rows(1)
+
+
+def finish(gate, partial, turned_a, turned_b, rows_a, rows_b, out_hbm, out, sem):
+    width = gate.shape[1]
+    tile = 2 * SPAN
+    copies = []
+    for j in range(width // tile):
+        at = slice(tile * j, tile * (j + 1))
+        first = partial[:, at] if at.stop <= partial.shape[1] else dot(rows_a[...], turned_a[:, at])
+        out[j] = (gate[:, at] * (first + dot(rows_b[...], turned_b[:, at]))).astype(jnp.bfloat16)
+        copies.append(pltpu.make_async_copy(out.at[j], out_hbm.at[:, pl.ds(tile * j, tile)], sem.at[j]))
+        copies[j].start()
+    for copy in copies:
+        copy.wait()
 
 
 def fused(tokens, w_mix, w_gate, gate_bias, w_branch):
@@ -303,31 +316,39 @@
     owner_sems = pltpu.SemaphoreType.DMA((2, n_dev // 2))
     device_sems = pltpu.SemaphoreType.DMA((n_dev,))
     vmem = lambda array: pltpu.VMEM(array.shape, array.dtype)
-    gate, partial, turned, rows = pl.pallas_call(
+    outs = pl.pallas_call(
         functools.partial(kernel, n_dev, n_col, 1.0 / math.sqrt(full_len * GROUP_DIM)),
         out_shape=[
             pltpu.VMEM((local_len, width), f32),
-            pltpu.VMEM((local_len, width), f32),
+            pltpu.VMEM((local_len, SPAN * 8), f32),
             pltpu.VMEM((SPAN, width), bf16),
+            pltpu.VMEM((SPAN, width), bf16),
+            pltpu.VMEM((local_len, SPAN), bf16),
             pltpu.VMEM((local_len, SPAN), bf16),
         ],
         in_specs=[any_space] * 12,
-        out_specs=[pl.BlockSpec(memory_space=pltpu.VMEM)] * 4,
+        out_specs=[pl.BlockSpec(memory_space=pltpu.VMEM)] * 6,
         scratch_shapes=[
             vmem(tokens), pltpu.VMEM((2, width, SPAN), bf16), vmem(w_gate), pltpu.VMEM((1, width), f32), vmem(w_branch),
             vmem(forward), vmem(back), vmem(first), vmem(cos_t), vmem(sin_t), vmem(last), vmem(perm),
             pltpu.VMEM((local_len, channels), bf16),
-            pltpu.VMEM((SPAN, width), bf16),
-            pltpu.VMEM((local_len, SPAN), bf16),
             by_owner, by_device, by_device, by_owner,
             pltpu.SemaphoreType.DMA((14,)),
             owner_sems, device_sems, device_sems, owner_sems,
         ],
         compiler_params=pltpu.CompilerParams(
-            collective_id=0, has_side_effects=True, vmem_limit_bytes=57_200_000
+            collective_id=0, has_side_effects=True, vmem_limit_bytes=55633280
         ),
     )(tokens, w_mix, w_gate, gate_bias.reshape(1, width), w_branch, *[jnp.asarray(t) for t in tables])
-    return (partial + gate * dot(rows, turned)).astype(bf16)
+    tiles = width // (2 * SPAN)
+    return pl.pallas_call(
+        finish,
+        out_shape=jax.ShapeDtypeStruct((local_len, width), bf16),
+        in_specs=[pl.BlockSpec(memory_space=pltpu.VMEM)] * 6,
+        out_specs=any_space,
+        scratch_shapes=[pltpu.VMEM((tiles, local_len, 2 * SPAN), bf16), pltpu.SemaphoreType.DMA((tiles,))],
+        compiler_params=pltpu.CompilerParams(vmem_limit_bytes=FINISH),
+    )(*outs)
 
 
 def shards(tokens, w_mix, w_gate, gate_bias, w_branch):

time: 34.3 us -> 32.4 us (0.945)
  matrix products: 2.04 us -> 0 us
    dot_general x1 -> x0, matrix products: 2.04 us -> none  [dot(): return jnp.dot(a, b, preferred_element_type=jnp.float32)]
    pallas_call x0 -> x1, Pallas kernels: none -> 1.65 us  [fused(): pl.pallas_call(finish, out_shape=jax.ShapeDtypeStruct((local_len, width),...]
    pallas_call x1, Pallas kernels: 32.1 us -> 30.6 us  [fused(): pl.pallas_call(functools.partial(kernel, n_dev, n_col, 1.0 / math.sqrt(fu...]
where the time goes in v3:
time: 32.4 us; the launch traced here: 32.2 us
  Pallas kernels  32.2 us (99%)
    pallas_call x1, Pallas kernels, fused(): pl.pallas_call(functools.partial(kernel, n_dev, n_col, 1.0 / math.sqrt(fu...  30.6 us
    pallas_call x1, Pallas kernels, fused(): pl.pallas_call(finish, out_shape=jax.ShapeDtypeStruct((local_len, width),...  1.65 us

profile of v3, /device:TPU:9, one launch (start us, length us, event | category | flops | bytes accessed | tf_op | source)
XLA Modules:
  0.0 32.2 jit_solution(1924270188532336172)
XLA Ops:
  0.0 30.6 %shard_map.118 = (f32[512,2048]{1,0:T(8,128)S(1)}, f32[512,2048]{1,0:T(8,128)S(1)}, bf16[256,2048]{1,0:T(8,128)(2,1)S(1)}, bf16[256,2048]{1,0:T(8,128)(2,1)S(1)}...) custom-call(bf16[512,2048]{1,0:T(8,128)(2,1)} %tok_hbm.1, bf16[2048,512]{1,0:T(8,128)(2,1)} %wmix_hbm.1, ...), custom_call_target="tpu_custom_call" | custom-call | tf_op jit(solution)/shard_map/pallas_call | solution.py:319
  30.6 1.7 %shard_map.119 = bf16[512,2048]{1,0:T(8,128)(2,1)} custom-call(f32[512,2048]{1,0:T(8,128)S(1)} %get-tuple-element.11.gate, f32[512,2048]{1,0:T(8,128)S(1)} %get-tuple-element.12.partial, bf16[256,2048]{1,0:T(8,128)(2,1)S(1)} %get-tuple-element.13.turned_a, bf16[256,2048]{1,0:T(8,128)(2,1)S(1)} %get-tuple-element.14.turned_b, ...), custom_call_target="tpu_custom_call" | custom-call | tf_op jit(solution)/shard_map/pallas_call | solution.py:344

commit v4 on v3

--- a/solution.py
+++ b/solution.py
@@ -133,7 +133,8 @@
         pl.semaphore_signal(barrier, inc=1, device_id=(peer // n_col, peer % n_col), device_id_type=MESH)
         return carry
 
-    lax.fori_loop(1, n, greet, 0)
+    for r in range(1, n):
+        greet(r, 0)
 
     def device(dev):
         return (dev // n_col, dev % n_col)
@@ -168,7 +169,7 @@
 
     def each_owner(h, act):
         def step(r, carry):
-            i = chip ^ ((r + 3 * owners // 4) % owners)
+            i = chip ^ ((r + (3 - 3 * h) * owners // 4) % owners)
 
             @pl.when(2 * i + h != me)
             def _():
@@ -278,13 +279,13 @@
 
 def finish(gate, partial, turned_a, turned_b, rows_a, rows_b, out_hbm, out, sem):
     width = gate.shape[1]
-    tile = 2 * SPAN
+    edges = (0, SPAN, 3 * SPAN, 5 * SPAN, 7 * SPAN, 8 * SPAN)
     copies = []
-    for j in range(width // tile):
-        at = slice(tile * j, tile * (j + 1))
+    for j, (lo, hi) in enumerate(zip(edges, edges[1:])):
+        at = slice(lo, hi)
         first = partial[:, at] if at.stop <= partial.shape[1] else dot(rows_a[...], turned_a[:, at])
-        out[j] = (gate[:, at] * (first + dot(rows_b[...], turned_b[:, at]))).astype(jnp.bfloat16)
-        copies.append(pltpu.make_async_copy(out.at[j], out_hbm.at[:, pl.ds(tile * j, tile)], sem.at[j]))
+        out[:, at] = (gate[:, at] * (first + dot(rows_b[...], turned_b[:, at]))).astype(jnp.bfloat16)
+        copies.append(pltpu.make_async_copy(out.at[:, at], out_hbm.at[:, at], sem.at[j]))
         copies[j].start()
     for copy in copies:
         copy.wait()
@@ -340,13 +341,12 @@
             collective_id=0, has_side_effects=True, vmem_limit_bytes=55633280
         ),
     )(tokens, w_mix, w_gate, gate_bias.reshape(1, width), w_branch, *[jnp.asarray(t) for t in tables])
-    tiles = width // (2 * SPAN)
     return pl.pallas_call(
         finish,
         out_shape=jax.ShapeDtypeStruct((local_len, width), bf16),
         in_specs=[pl.BlockSpec(memory_space=pltpu.VMEM)] * 6,
         out_specs=any_space,
-        scratch_shapes=[pltpu.VMEM((tiles, local_len, 2 * SPAN), bf16), pltpu.SemaphoreType.DMA((tiles,))],
+        scratch_shapes=[pltpu.VMEM((local_len, width), bf16), pltpu.SemaphoreType.DMA((5,))],
         compiler_params=pltpu.CompilerParams(vmem_limit_bytes=FINISH),
     )(*outs)
 

time: 32.4 us -> 32.5 us (level)
  no operation moved by 1% of the time
where the time goes in v4:
time: 32.5 us; the launch traced here: 32.4 us
  Pallas kernels  32.4 us (100%)
    pallas_call x1, Pallas kernels, fused(): pl.pallas_call(functools.partial(kernel, n_dev, n_col, 1.0 / math.sqrt(fu...  30.6 us
    pallas_call x1, Pallas kernels, fused(): pl.pallas_call(finish, out_shape=jax.ShapeDtypeStruct((local_len, width),...  1.82 us

profile of v4, /device:TPU:9, one launch (start us, length us, event | category | flops | bytes accessed | tf_op | source)
XLA Modules:
  0.0 32.4 jit_solution(7238772434720216393)
XLA Ops:
  0.0 30.6 %shard_map.118 = (f32[512,2048]{1,0:T(8,128)S(1)}, f32[512,2048]{1,0:T(8,128)S(1)}, bf16[256,2048]{1,0:T(8,128)(2,1)S(1)}, bf16[256,2048]{1,0:T(8,128)(2,1)S(1)}...) custom-call(bf16[512,2048]{1,0:T(8,128)(2,1)} %tok_hbm.1, bf16[2048,512]{1,0:T(8,128)(2,1)} %wmix_hbm.1, ...), custom_call_target="tpu_custom_call" | custom-call | tf_op jit(solution)/shard_map/pallas_call | solution.py:320
  30.6 1.8 %shard_map.119 = bf16[512,2048]{1,0:T(8,128)(2,1)} custom-call(f32[512,2048]{1,0:T(8,128)S(1)} %get-tuple-element.11.gate, f32[512,2048]{1,0:T(8,128)S(1)} %get-tuple-element.12.partial, bf16[256,2048]{1,0:T(8,128)(2,1)S(1)} %get-tuple-element.13.turned_a, bf16[256,2048]{1,0:T(8,128)(2,1)S(1)} %get-tuple-element.14.turned_b, ...), custom_call_target="tpu_custom_call" | custom-call | tf_op jit(solution)/shard_map/pallas_call | solution.py:344
